TPU v7x, 32 devices: a whole 2x2x4 slice. The times are simulated.
32 devices in a mesh: grp: 2 (over x), tp: 4 (over y, core), dp: 4 (over z).
Axes of the slice: x: 2, y: 2, z: 4, core: 2. Of those that a mesh axis runs over, the one named last changes fastest.
Arguments:
- tokens: bfloat16 [512, 2048], P(('grp', 'tp'), 'dp'), parts along dimension 0, may hold values from -25 to 25
- state: float32 [2, 512, 16, 128, 128], P(None, ('grp', 'dp'), 'tp'), parts along dimension 1, may hold values from -1 to 1
- lengths: int32 [512], P(('grp', 'dp')), parts along dimension 0, may hold values from 1 to 4096, 131072 in all
- norm_gain: bfloat16 [2, 2048], P(None, 'dp'), may hold values from 0.099609375 to 1.8984375
- w_query: bfloat16 [2, 2048, 2048], P(None, 'dp', 'tp'), may hold values from -0.125 to 0.125
- w_forget: bfloat16 [2, 2048, 2048], P(None, 'dp', 'tp'), may hold values from -0.125 to 0.125
- w_input: bfloat16 [2, 2048, 2048], P(None, 'dp', 'tp'), may hold values from -0.125 to 0.125
- w_gate: bfloat16 [2, 2048, 2048], P(None, 'dp', 'tp'), may hold values from -0.125 to 0.125
- w_out: bfloat16 [2, 2048, 2048], P(None, 'tp', 'dp'), may hold values from -0.125 to 0.125
- bound_logit: float32 [2, 2048], P(None, 'tp'), may hold values from -3 to 5
- pace: float32 [2, 2048], P(None, 'tp'), may hold values from 0.6 to 2
- head_gain: float32 [2, 128], replicated, may hold values from 0.4 to 2.5
Outputs:
- mixed: float32 [512, 2048], P(('grp', 'tp'), 'dp'), parts along dimension 0
- new_state: float32 [2, 512, 16, 128, 128], P(None, ('grp', 'dp'), 'tp'), parts along dimension 1
There are 2 independent parts, one for each index of `grp`. A program takes and returns all parts, laid end to end along the dimension named above; an argument that names none is the same for every part. Nothing has to cross between parts.
All inputs are finite; a program needn't handle non-finite values. No bound on the sum of `lengths` on one device may be relied on, other than what follows from the above.
Results may differ from a plain program's by a relative error of at most 0.0083.
Values may be sent and summed in bfloat16 or wider, within the bound.
A program may use at most 192 MiB of HBM per device.

v0:
```python
import jax
import jax.numpy as jnp
from jax import lax
from jax.sharding import PartitionSpec as P

D = 2048
LENGTH_MEAN = 512


epsilon = 1e-06


def advance(prior, query, forget_in, value, gate, lower, pace_row, log_len, gain_row):
    count, width = query.shape
    size = prior.shape[-1]
    heads = width // size
    pre = forget_in - pace_row[None, :] * log_len[:, None]
    forget = lower[None, :] + (1.0 - lower[None, :]) * jax.nn.sigmoid(pre)
    key = (1.0 - lower[None, :]) * jax.nn.sigmoid(-pre)
    forget = forget.reshape(count, heads, size)
    key = key.reshape(count, heads, size)
    values = value.reshape(count, heads, size)
    updated = forget[..., None] * prior + key[..., None] * values[:, :, None, :]
    readout = jnp.einsum(
        "bhk,bhkv->bhv", query.reshape(count, heads, size), updated, precision=lax.Precision.HIGHEST
    )
    normed = readout * lax.rsqrt(jnp.mean(readout * readout, axis=-1, keepdims=True) + epsilon)
    gates = gate.reshape(count, heads, size)
    normed = normed * gain_row[None, None, :] * jax.nn.silu(gates)
    return (updated, normed.reshape(count, width).astype(jnp.bfloat16))


def shards(
    tokens,
    state,
    lengths,
    norm_gain,
    w_query,
    w_forget,
    w_input,
    w_gate,
    w_out,
    bound_logit,
    pace,
    head_gain,
):
    current = tokens
    log_len = jnp.log(lengths.astype(jnp.float32) / LENGTH_MEAN)
    own_count = state.shape[1]
    states = []
    result = None
    for block in range(2):
        whole = lax.all_gather(current, "tp", axis=0, tiled=True)
        whole_wide = whole.astype(jnp.float32)
        partial_sq = jnp.sum(whole_wide * whole_wide, axis=1)
        squares_all = lax.psum(partial_sq, "dp")
        squares = lax.dynamic_slice_in_dim(
            squares_all, lax.axis_index("dp") * own_count, own_count, 0
        )
        gained = (whole_wide * norm_gain[block].astype(jnp.float32)[None, :]).astype(jnp.bfloat16)
        terms = tuple(
            (
                jnp.dot(gained, weight[block], preferred_element_type=jnp.float32)
                for weight in (w_query, w_forget, w_input, w_gate)
            )
        )
        sums = lax.psum_scatter(terms, "dp", scatter_dimension=0, tiled=True)
        scale = lax.rsqrt(squares / D + epsilon)
        made = [scale[:, None] * total for total in sums]
        lower = jax.nn.sigmoid(bound_logit[block])
        updated, normed = advance(
            state[block],
            made[0],
            made[1],
            made[2],
            made[3],
            lower,
            pace[block],
            log_len,
            head_gain[block],
        )
        states.append(updated)
        gathered = lax.all_gather(normed, "dp", axis=0, tiled=True)
        out_weight = w_out[block]
        branch = lax.psum_scatter(
            jnp.dot(gathered, out_weight, preferred_element_type=jnp.float32),
            "tp",
            scatter_dimension=0,
            tiled=True,
        )
        if block == 0:
            current = (current.astype(jnp.float32) + branch).astype(jnp.bfloat16)
        else:
            result = current.astype(jnp.float32) + branch
    return (result, jnp.stack(states))


def solution(mesh):
    in_specs = (
        P(("grp", "tp"), "dp"),
        P(None, ("grp", "dp"), "tp", None, None),
        P(("grp", "dp")),
        P(None, "dp"),
        P(None, "dp", "tp"),
        P(None, "dp", "tp"),
        P(None, "dp", "tp"),
        P(None, "dp", "tp"),
        P(None, "tp", "dp"),
        P(None, "tp"),
        P(None, "tp"),
        P(),
    )
    out_specs = (P(("grp", "tp"), "dp"), P(None, ("grp", "dp"), "tp", None, None))
    return jax.shard_map(shards, mesh=mesh, in_specs=in_specs, out_specs=out_specs, check_vma=False)
```

profile of v0, /device:TPU:0, one launch (start us, length us, event | category | flops | bytes accessed | tf_op | source)
XLA Modules:
  0.0 361.6 jit_solution(16375477499638168452)
XLA Ops:
  7.2 0.0 reduce-scatter.13.cloned.1.call-start
  7.2 0.8 slice_convert_fusion
  8.0 7.4 %all_gather.12 = bf16[256,512]{1,0:T(8,128)(2,1)S(1)} all-gather(bf16[64,512]{1,0:T(8,128)(2,1)} %param.12), channel_id=1, replica_groups=mesh['grp'=2,'tp'=4,'dp'=4] {'tp'}, dimensions={0}, use_global_device_ids=true | all-gather | bytes 327680 | tf_op jit(solution)/shard_map/all_gather | solution.py:53
  15.4 2.1 fusion.36
  17.6 0.0 reduce-scatter.13.cloned.1.call-update
  17.6 0.0 reduce-scatter.15.cloned.1.call-start
  17.6 2.1 fusion.34
  19.8 0.0 reduce-scatter.15.cloned.1.call-update
  19.8 0.0 reduce-scatter.17.cloned.1.call-start
  19.8 2.2 fusion.32
  22.0 0.0 reduce-scatter.17.cloned.1.call-update
  22.0 0.0 reduce-scatter.11.cloned.1.call-start
  22.1 2.2 fusion.38
  24.2 0.0 reduce-scatter.11.cloned.1.call-update
  24.3 0.0 reduce-scatter.19.cloned.1.call-start
  24.3 0.1 fusion.16
  24.5 12.0 %psum.14 = f32[256]{0:T(256)S(1)} all-reduce(f32[256]{0:T(256)S(1)} %fusion.16), channel_id=1, replica_groups=mesh['grp'=2,'tp'=4,'dp'=4] {'dp'}, use_global_device_ids=true, to_apply=%region_1.0 | all-reduce | flops 256 | bytes 2048 | tf_op jit(solution)/shard_map/psum | solution.py:56
  36.4 0.1 add_rsqrt_fusion.3
  36.5 0.7 multiply_log_fusion
  37.2 1.3 slice_bitcast_fusion
  38.5 0.8 fusion.62
  39.3 0.8 broadcast_subtract_fusion
  40.1 0.8 reduce-scatter.13.cloned.1.call-done
  40.9 22.4 %reduce-scatter.15.cloned.1.call-done = f32[64,512]{1,0:T(8,128)} async-done(((f32[256,512]{1,0:T(8,128)}), f32[64,512]{1,0:T(8,128)}) %reduce-scatter.15.cloned.1.call-update) | async-done | bytes 131088 | tf_op jit(solution)/shard_map/reduce_scatter | solution.py:67
  63.4 22.4 %reduce-scatter.17.cloned.1.call-done = f32[64,512]{1,0:T(8,128)} async-done(((f32[256,512]{1,0:T(8,128)}), f32[64,512]{1,0:T(8,128)}) %reduce-scatter.17.cloned.1.call-update) | async-done | bytes 131088 | tf_op jit(solution)/shard_map/reduce_scatter | solution.py:67
  85.8 22.2 %reduce-scatter.11.cloned.1.call-done = f32[64,512]{1,0:T(8,128)} async-done(((f32[256,512]{1,0:T(8,128)}), f32[64,512]{1,0:T(8,128)}) %reduce-scatter.11.cloned.1.call-update) | async-done | bytes 131088 | tf_op jit(solution)/shard_map/reduce_scatter | solution.py:67
  108.0 1.2 multiply_add_fusion.3
  109.5 0.7 reshape.56
  110.2 0.7 reshape.61
  110.9 22.7 %fusion.4 = f32[64,4,1,128]{3,2,1,0:T(1,128)S(1)} fusion(f32[64,4,128,1]{2,3,1,0:T(1,128)} %bitcast.79, f32[2,64,4,128,128]{4,3,2,1,0:T(8,128)} %param.13, f32[64,4,128]{2,1,0:T(4,128)S(1)} %mul.316, f32[64,4,128]{2,1,0:T(4,128)S(1)} %mul.313, f32[64,4,128]{2,1,0:T(4,128)S(1)} %mul.309), kind=kOutput, calls=%fused_computation.6 | convolution fusion | flops 62914560 | bytes 17432576 | tf_op jit(solution)/shard_map/bhk,bhkv->bhv/dot_general | solution.py:24
  133.6 0.1 multiply_reduce_fusion.1
  133.8 0.1 fusion.61
  134.0 13.8 %all_gather.13 = bf16[256,512]{1,0:T(8,128)(2,1)S(1)} all-gather(bf16[64,512]{1,0:T(8,128)(2,1)S(1)} %bitcast.74), channel_id=1, replica_groups=mesh['grp'=2,'tp'=4,'dp'=4] {'dp'}, dimensions={0}, use_global_device_ids=true | all-gather | bytes 327680 | tf_op jit(solution)/shard_map/all_gather | solution.py:83
  147.8 2.1 fusion.30
  149.9 0.0 reduce-scatter.19.cloned.1.call-update
  150.0 0.0 reduce-scatter.23.cloned.1.call-start
  150.0 19.9 %reduce-scatter.19.cloned.1.call-done = f32[64,512]{1,0:T(8,128)} async-done(((f32[256,512]{1,0:T(8,128)}), f32[64,512]{1,0:T(8,128)}) %reduce-scatter.19.cloned.1.call-update) | async-done | bytes 131088 | tf_op jit(solution)/shard_map/reduce_scatter | solution.py:85
  169.9 0.9 add_convert_fusion
  170.9 5.8 %all_gather.14 = bf16[256,512]{1,0:T(8,128)(2,1)S(1)} all-gather(bf16[64,512]{1,0:T(8,128)(2,1)S(1)} %add_convert_fusion), channel_id=1, replica_groups=mesh['grp'=2,'tp'=4,'dp'=4] {'tp'}, dimensions={0}, use_global_device_ids=true | all-gather | bytes 327680 | tf_op jit(solution)/shard_map/all_gather | solution.py:53
  176.7 1.1 fusion.26
  177.8 0.0 reduce-scatter.23.cloned.1.call-update
  177.8 0.0 reduce-scatter.25.cloned.1.call-start
  177.8 1.1 fusion.24
  178.9 0.0 reduce-scatter.27.cloned.1.call-start
  179.0 1.1 fusion.22
  180.1 0.0 reduce-scatter.21.cloned.1.call-start
  180.2 2.2 fusion.28
  182.4 0.0 reduce-scatter.29.cloned.1.call-start
  182.4 0.1 fusion.18
  182.6 11.7 %psum.15 = f32[256]{0:T(256)S(1)} all-reduce(f32[256]{0:T(256)S(1)} %fusion.18), channel_id=1, replica_groups=mesh['grp'=2,'tp'=4,'dp'=4] {'dp'}, use_global_device_ids=true, to_apply=%region_9.10 | all-reduce | flops 256 | bytes 2048 | tf_op jit(solution)/shard_map/psum | solution.py:56
  194.3 0.1 add_rsqrt_fusion.2
  194.4 5.5 %reduce-scatter.23.cloned.1.call-done = f32[64,512]{1,0:T(8,128)} async-done(((f32[256,512]{1,0:T(8,128)}), f32[64,512]{1,0:T(8,128)}) %reduce-scatter.23.cloned.1.call-update) | async-done | bytes 131088 | tf_op jit(solution)/shard_map/reduce_scatter | solution.py:67
  199.9 22.4 %reduce-scatter.25.cloned.1.call-done = f32[64,512]{1,0:T(8,128)} async-done(((f32[256,512]{1,0:T(8,128)}), f32[64,512]{1,0:T(8,128)}) %reduce-scatter.25.cloned.1.call-update) | async-done | bytes 131088 | tf_op jit(solution)/shard_map/reduce_scatter | solution.py:67
  222.3 22.4 %reduce-scatter.27.cloned.1.call-done = f32[64,512]{1,0:T(8,128)} async-done(((f32[256,512]{1,0:T(8,128)}), f32[64,512]{1,0:T(8,128)}) %reduce-scatter.27.cloned.1.call-update) | async-done | bytes 131088 | tf_op jit(solution)/shard_map/reduce_scatter | solution.py:67
  244.7 22.4 %reduce-scatter.21.cloned.1.call-done = f32[64,512]{1,0:T(8,128)} async-done(((f32[256,512]{1,0:T(8,128)}), f32[64,512]{1,0:T(8,128)}) %reduce-scatter.21.cloned.1.call-update) | async-done | bytes 131088 | tf_op jit(solution)/shard_map/reduce_scatter | solution.py:67
  267.1 1.2 multiply_add_fusion.2
  268.6 23.2 %multiply_add_fusion.1 = (f32[1,64,4,128,128]{4,3,2,1,0:T(8,128)}, f32[1,64,4,128,128]{4,3,2,1,0:T(8,128)}) fusion(f32[2,64,4,128,128]{4,3,2,1,0:T(8,128)} %param.13, f32[64,4,128]{2,1,0:T(4,128)} %copy-done.6, f32[64,4,128]{2,1,0:T(4,128)} %copy-done.5, f32[64,4,128]{2,1,0:T(4,128)} %copy-done.4, f32[64,4,128]{2,1,0:T(4,128)S(1)} %mul.349, ...), kind=kLoop, calls=%fused_computation.8 | loop fusion | flops 25165824 | bytes 67895296 | tf_op jit(solution)/shard_map/add | solution.py:23
  291.8 22.6 %fusion.1 = f32[64,4,1,128]{3,2,1,0:T(1,128)S(1)} fusion(f32[64,4,128,1]{2,3,1,0:T(1,128)S(1)} %bitcast.78, f32[2,64,4,128,128]{4,3,2,1,0:T(8,128)} %param.13, f32[64,4,128]{2,1,0:T(4,128)S(1)} %mul.349, f32[64,4,128]{2,1,0:T(4,128)S(1)} %mul.346, f32[64,4,128]{2,1,0:T(4,128)S(1)} %mul.342), kind=kOutput, calls=%fused_computation.3 | convolution fusion | flops 62914560 | bytes 17432576 | tf_op jit(solution)/shard_map/bhk,bhkv->bhv/dot_general | solution.py:24
  314.4 0.1 multiply_reduce_fusion
  314.6 0.1 fusion.60
  314.8 13.8 %all_gather.15 = bf16[256,512]{1,0:T(8,128)(2,1)S(1)} all-gather(bf16[64,512]{1,0:T(8,128)(2,1)S(1)} %bitcast.75), channel_id=1, replica_groups=mesh['grp'=2,'tp'=4,'dp'=4] {'dp'}, dimensions={0}, use_global_device_ids=true | all-gather | bytes 327680 | tf_op jit(solution)/shard_map/all_gather | solution.py:83
  328.6 1.1 fusion.20
  329.7 23.4 %pad_maximum_fusion = f32[2,64,4,128,128]{4,3,2,1,0:T(8,128)} fusion(f32[1,64,4,128,128]{4,3,2,1,0:T(8,128)} %get-tuple-element.7, f32[1,64,4,128,128]{4,3,2,1,0:T(8,128)} %get-tuple-element.6), kind=kLoop, calls=%fused_computation | loop fusion | flops 8388608 | bytes 67108864 | tf_op jit(solution)/shard_map/stack | solution.py:95
  353.1 1.6 convert_add_fusion
  (39 shorter events, 0.5 us)
Async XLA Ops:
  7.2 33.7 %reduce-scatter.13.cloned.1.call-start = ((), (), s32[]{:S(2)}) async-start(), calls=%async_computation.11 | async-start | bytes 655360 | tf_op jit(solution)/shard_map/reduce_scatter | solution.py:67
  17.6 45.8 %reduce-scatter.15.cloned.1.call-start = ((), (), s32[]{:S(2)}) async-start(), calls=%async_computation.12 | async-start | bytes 655360 | tf_op jit(solution)/shard_map/reduce_scatter | solution.py:67
  19.8 66.0 %reduce-scatter.17.cloned.1.call-start = ((), (), s32[]{:S(2)}) async-start(), calls=%async_computation.13 | async-start | bytes 655360 | tf_op jit(solution)/shard_map/reduce_scatter | solution.py:67
  22.0 86.0 %reduce-scatter.11.cloned.1.call-start = ((), (), s32[]{:S(2)}) async-start(), calls=%async_computation.10 | async-start | bytes 655360 | tf_op jit(solution)/shard_map/reduce_scatter | solution.py:67
  24.3 145.7 %reduce-scatter.19.cloned.1.call-start = ((), (), s32[]{:S(2)}) async-start(), calls=%async_computation.14 | async-start | bytes 655360 | tf_op jit(solution)/shard_map/reduce_scatter | solution.py:85
  37.2 73.7 %copy-start.8 = (f32[64]{0:T(128)}, f32[64]{0:T(128)S(1)}, u32[]{:S(2)}) copy-start(f32[64]{0:T(128)S(1)} %multiply_log_fusion) | copy-start | bytes 772
  109.3 24.6 %copy-start.4 = (f32[64,4,128]{2,1,0:T(4,128)}, f32[64,4,128]{2,1,0:T(4,128)S(1)}, u32[]{:S(2)}) copy-start(f32[64,4,128]{2,1,0:T(4,128)S(1)} %mul.309) | copy-start | bytes 393220
  109.4 24.6 %copy-start.5 = (f32[64,4,128]{2,1,0:T(4,128)}, f32[64,4,128]{2,1,0:T(4,128)S(1)}, u32[]{:S(2)}) copy-start(f32[64,4,128]{2,1,0:T(4,128)S(1)} %mul.313) | copy-start | bytes 393220
  109.5 40.5 %copy-start.6 = (f32[64,4,128]{2,1,0:T(4,128)}, f32[64,4,128]{2,1,0:T(4,128)S(1)}, u32[]{:S(2)}) copy-start(f32[64,4,128]{2,1,0:T(4,128)S(1)} %mul.316) | copy-start | bytes 393220
  110.9 22.9 %copy-start.7 = (f32[64,4,128]{2,1,0:T(4,128)S(1)}, f32[64,4,128]{2,1,0:T(4,128)}, u32[]{:S(2)}) copy-start(f32[64,4,128]{2,1,0:T(4,128)} %reshape.56) | copy-start | bytes 393220
  110.9 22.9 %copy-start.10 = (f32[128]{0:T(128)S(1)}, f32[128]{0:T(128)}, u32[]{:S(2)}) copy-start(f32[128]{0:T(128)} %get-tuple-element.19) | copy-start | bytes 1540
  110.9 65.8 %copy-start = (bf16[2,512,512]{2,1,0:T(8,128)(2,1)S(1)}, bf16[2,512,512]{2,1,0:T(8,128)(2,1)}, u32[]{:S(2)}) copy-start(bf16[2,512,512]{2,1,0:T(8,128)(2,1)} %param.17) | copy-start | bytes 3145732
  110.9 66.9 %copy-start.1 = (bf16[2,512,512]{2,1,0:T(8,128)(2,1)S(1)}, bf16[2,512,512]{2,1,0:T(8,128)(2,1)}, u32[]{:S(2)}) copy-start(bf16[2,512,512]{2,1,0:T(8,128)(2,1)} %param.18) | copy-start | bytes 3145732
  110.9 68.1 %copy-start.2 = (bf16[2,512,512]{2,1,0:T(8,128)(2,1)S(1)}, bf16[2,512,512]{2,1,0:T(8,128)(2,1)}, u32[]{:S(2)}) copy-start(bf16[2,512,512]{2,1,0:T(8,128)(2,1)} %param.19) | copy-start | bytes 3145732
  150.0 49.9 %reduce-scatter.23.cloned.1.call-start = ((), (), s32[]{:S(2)}) async-start(), calls=%async_computation.16 | async-start | bytes 655360 | tf_op jit(solution)/shard_map/reduce_scatter | solution.py:67
  177.8 44.5 %reduce-scatter.25.cloned.1.call-start = ((), (), s32[]{:S(2)}) async-start(), calls=%async_computation.17 | async-start | bytes 655360 | tf_op jit(solution)/shard_map/reduce_scatter | solution.py:67
  178.9 65.7 %reduce-scatter.27.cloned.1.call-start = ((), (), s32[]{:S(2)}) async-start(), calls=%async_computation.18 | async-start | bytes 655360 | tf_op jit(solution)/shard_map/reduce_scatter | solution.py:67
  180.1 86.9 %reduce-scatter.21.cloned.1.call-start = ((), (), s32[]{:S(2)}) async-start(), calls=%async_computation.15 | async-start | bytes 655360 | tf_op jit(solution)/shard_map/reduce_scatter | solution.py:67
  182.4 170.8 %reduce-scatter.29.cloned.1.call-start = ((), (), s32[]{:S(2)}) async-start(), calls=%async_computation.19 | async-start | bytes 655360 | tf_op jit(solution)/shard_map/reduce_scatter | solution.py:85
  291.8 22.8 %copy-start.9 = (f32[128]{0:T(128)S(1)}, f32[128]{0:T(128)}, u32[]{:S(2)}) copy-start(f32[128]{0:T(128)} %get-tuple-element.18) | copy-start | bytes 1540
  291.8 36.8 %copy-start.3 = (bf16[2,512,512]{2,1,0:T(8,128)(2,1)S(1)}, bf16[2,512,512]{2,1,0:T(8,128)(2,1)}, u32[]{:S(2)}) copy-start(bf16[2,512,512]{2,1,0:T(8,128)(2,1)} %param.20) | copy-start | bytes 3145732
Sparse Core Ops, SparseCore 0:
  17.7 23.1 reduce-scatter.12
  43.2 20.1 reduce-scatter.14
  65.6 20.1 reduce-scatter.16
  87.9 20.0 reduce-scatter.10
  150.1 19.8 reduce-scatter.18
  177.9 21.9 reduce-scatter.22
  202.2 20.0 reduce-scatter.24
  224.6 20.0 reduce-scatter.26
  247.0 20.0 reduce-scatter.20
  329.8 19.8 reduce-scatter.28
where the time goes:
time: 362 us
  waiting for transfers between devices  161 us (44%)
  blocking collectives  64.5 us (18%)
  matrix products  62.6 us (17%)
  other arithmetic  54.8 us (15%)
  between operations  14.5 us (4%)
  local copies, waits for them, and re-layouts  3.97 us (1%)
    reduce_scatter x8, waiting for transfers between devices, shards(): sums = lax.psum_scatter(terms, 'dp', scatter_dimension=0, tiled=True)  141 us
    dot_general x2, matrix products, advance(): jnp.einsum('bhk,bhkv->bhv', query.reshape(count, heads, size), updated, p...  45.3 us
    all_gather x2, blocking collectives, shards(): gathered = lax.all_gather(normed, 'dp', axis=0, tiled=True)  27.6 us
    psum x2, blocking collectives, shards(): squares_all = lax.psum(partial_sq, 'dp')  23.7 us
    another operation x1, other arithmetic, shards(): return (result, jnp.stack(states))  23.4 us
    add x1, other arithmetic, advance(): updated = forget[..., None] * prior + key[..., None] * values[:, :, None, :]  23.2 us
    reduce_scatter x2, waiting for transfers between devices, shards(): lax.psum_scatter(jnp.dot(gathered, out_weight, preferred_element_type=jnp...  19.9 us
    dot_general x8, matrix products, shards(): jnp.dot(gained, weight[block], preferred_element_type=jnp.float32)  14.1 us
  transfers between devices with their start and end apart: 10, of which 9 were waited for; matrix products, arithmetic and copies ran while one was open for 11% of the time, Pallas kernels for 0%

commit v1 on v0

v1 whole, which is shorter than its diff:
```python
import functools

import jax
import jax.numpy as jnp
from jax import lax
from jax.experimental import pallas as pl
from jax.experimental.pallas import tpu as pltpu
from jax.sharding import PartitionSpec as P

LENGTH_MEAN = 512
epsilon = 1e-06
GROUP = 8
MESH_ID = pl.DeviceIdType.MESH
f32 = jnp.float32
bf16 = jnp.bfloat16


def chain(
    n_tp,
    n_dp,
    width,
    tokens,
    state,
    lengths,
    gain,
    w_query,
    w_forget,
    w_input,
    w_gate,
    w_out,
    bound,
    pace,
    head_gain,
    mixed,
    forget_o,
    key_o,
    value_o,
    xall,
    sbuf,
    wbuf,
    wobuf,
    psend,
    precv,
    pown,
    nall,
    osend,
    orecv,
    oown,
    gate_s,
    qf_s,
    qk_s,
    ro_s,
    w_sem,
    s_sem,
    x_ss,
    x_rs,
    p_ss,
    p_rs,
    n_ss,
    n_rs,
    o_ss,
    o_rs,
):
    t, d = lax.axis_index("tp"), lax.axis_index("dp")
    rt, feats = tokens.shape
    own, heads, size = state.shape[1], state.shape[2], state.shape[3]
    chans = heads * size
    groups = own // GROUP

    def tp_peer(k):
        return lax.rem(t + k, n_tp)

    def dp_peer(k):
        return lax.rem(d + k, n_dp)

    loads = []
    for b in range(2):
        per = []
        for i, w in enumerate((w_query, w_forget, w_input, w_gate)):
            per.append(pltpu.make_async_copy(w.at[b], wbuf.at[b, i], w_sem.at[b, i]))
        per.append(pltpu.make_async_copy(w_out.at[b], wobuf.at[b], w_sem.at[b, 4]))
        loads.append(per)

    def state_load(b, g):
        rows = pl.ds(g * GROUP, GROUP)
        return pltpu.make_async_copy(state.at[b, rows], sbuf.at[b, rows], s_sem.at[b, g])

    for c in loads[0]:
        c.start()

    barrier = pltpu.get_barrier_semaphore()
    for k in range(1, n_tp):
        pl.semaphore_signal(barrier, inc=1, device_id={"tp": tp_peer(k)}, device_id_type=MESH_ID)
    for k in range(1, n_dp):
        pl.semaphore_signal(barrier, inc=1, device_id={"dp": dp_peer(k)}, device_id_type=MESH_ID)
    pl.semaphore_wait(barrier, n_tp + n_dp - 2)

    my_rows = pl.ds(pl.multiple_of(t * rt, rt), rt)
    my_seqs = pl.ds(pl.multiple_of(d * own, own), own)
    sends = []
    current = tokens[...].astype(f32)
    log_len = jnp.log(lengths[...].astype(f32) / LENGTH_MEAN)
    lane = lax.broadcasted_iota(jnp.int32, (own, 128), 1)
    row_id = lax.broadcasted_iota(jnp.int32, (GROUP, size), 0)

    for b in range(2):
        copies = []
        for k in range(1, n_tp):
            c = pltpu.make_async_remote_copy(
                src_ref=tokens if b == 0 else xall.at[b, my_rows],
                dst_ref=xall.at[b, my_rows],
                send_sem=x_ss.at[b, k - 1],
                recv_sem=x_rs.at[b, k - 1],
                device_id={"tp": tp_peer(k)},
                device_id_type=MESH_ID,
            )
            c.start()
            copies.append(c)
        sends += copies
        if b == 0:
            xall[b, my_rows, :] = tokens[...]
            for g in range(groups):
                state_load(0, g).start()
            for c in loads[1]:
                c.start()
            for g in range(groups):
                state_load(1, g).start()
        for i in range(4):
            loads[b][i].wait()
        for c in copies:
            c.wait_recv()

        gain_row = gain[b : b + 1, :].astype(f32)
        copies = []
        for k in [n_dp // 2] + [k for k in range(1, n_dp) if k != n_dp // 2] + [0]:
            dest = dp_peer(k)
            x = xall[b, pl.ds(pl.multiple_of(dest * own, own), own), :].astype(f32)
            sq = jnp.sum(x * x, axis=1, keepdims=True)
            gained = (x * gain_row).astype(bf16)
            for i in range(4):
                part = jnp.dot(gained, wbuf[b, i], preferred_element_type=f32)
                if k == 0:
                    pown[:, i * chans : (i + 1) * chans] = part
                else:
                    psend[b, k - 1, :, i * chans : (i + 1) * chans] = part.astype(bf16)
            if k == 0:
                own_sq = sq
            else:
                hi = sq.astype(bf16).astype(f32)
                packed = jnp.where(lane == 0, hi, jnp.where(lane == 1, sq - hi, 0.0))
                psend[b, k - 1, :, 4 * chans :] = packed.astype(bf16)
                c = pltpu.make_async_remote_copy(
                    src_ref=psend.at[b, k - 1],
                    dst_ref=precv.at[b, k - 1],
                    send_sem=p_ss.at[b, k - 1],
                    recv_sem=p_rs.at[b, k - 1],
                    device_id={"dp": dest},
                    device_id_type=MESH_ID,
                )
                c.start()
                copies.append(c)
        sends += copies
        for c in copies:
            c.wait_recv()

        squares = own_sq
        for k in range(n_dp - 1):
            squares = squares + jnp.sum(precv[b, k, :, 4 * chans :].astype(f32), axis=1, keepdims=True)
        scale = lax.rsqrt(squares / width + epsilon)

        def total(i):
            cols = slice(i * chans, (i + 1) * chans)
            acc = pown[:, cols]
            for k in range(n_dp - 1):
                acc = acc + precv[b, k, :, cols].astype(f32)
            return scale * acc

        lower = jax.nn.sigmoid(bound[b : b + 1, :])
        pre = total(1) - pace[b : b + 1, :] * log_len
        forget = lower + (1.0 - lower) * jax.nn.sigmoid(pre)
        key = (1.0 - lower) * jax.nn.sigmoid(-pre)
        forget_o[b] = forget
        key_o[b] = key
        query = total(0)
        qf_s[...] = query * forget
        qk_s[...] = query * key
        value_o[b] = total(2)
        gate = total(3)
        gate_s[...] = gate * jax.nn.sigmoid(gate)

        for g in range(groups):
            state_load(b, g).wait()

        def read(g, carry):
            rows = pl.ds(pl.multiple_of(g * GROUP, GROUP), GROUP)
            for h in range(heads):
                cols = slice(h * size, (h + 1) * size)
                q8 = qf_s[rows, cols]
                diag = jnp.concatenate(
                    [jnp.where(row_id == j, q8, 0.0) for j in range(GROUP)], axis=1
                ).astype(bf16)
                s8 = sbuf[b, rows, h].reshape(GROUP * size, size).astype(bf16)
                ro_s[rows, cols] = jnp.dot(diag, s8, preferred_element_type=f32)
            return carry

        lax.fori_loop(0, groups, read, 0)
        for h in range(heads):
            cols = slice(h * size, (h + 1) * size)
            dots = jnp.sum(qk_s[:, cols], axis=1, keepdims=True)
            readout = ro_s[:, cols] + dots * value_o[b, :, cols]
            mean = jnp.mean(readout * readout, axis=1, keepdims=True)
            normed = readout * lax.rsqrt(mean + epsilon) * head_gain[b : b + 1, :] * gate_s[:, cols]
            nall[b, my_seqs, cols] = normed.astype(bf16)

        copies = []
        for k in range(1, n_dp):
            c = pltpu.make_async_remote_copy(
                src_ref=nall.at[b, my_seqs],
                dst_ref=nall.at[b, my_seqs],
                send_sem=n_ss.at[b, k - 1],
                recv_sem=n_rs.at[b, k - 1],
                device_id={"dp": dp_peer(k)},
                device_id_type=MESH_ID,
            )
            c.start()
            copies.append(c)
        sends += copies
        loads[b][4].wait()
        for c in copies:
            c.wait_recv()

        copies = []
        for k in list(range(1, n_tp)) + [0]:
            dest = tp_peer(k)
            rows = nall[b, pl.ds(pl.multiple_of(dest * rt, rt), rt), :]
            part = jnp.dot(rows, wobuf[b], preferred_element_type=f32)
            if k == 0:
                oown[...] = part
            else:
                osend[b, k - 1] = part.astype(bf16)
                c = pltpu.make_async_remote_copy(
                    src_ref=osend.at[b, k - 1],
                    dst_ref=orecv.at[b, k - 1],
                    send_sem=o_ss.at[b, k - 1],
                    recv_sem=o_rs.at[b, k - 1],
                    device_id={"tp": dest},
                    device_id_type=MESH_ID,
                )
                c.start()
                copies.append(c)
        sends += copies
        for c in copies:
            c.wait_recv()
        branch = oown[...]
        for k in range(n_tp - 1):
            branch = branch + orecv[b, k].astype(f32)
        if b == 0:
            rounded = (current + branch).astype(bf16)
            xall[1, my_rows, :] = rounded
            current = rounded.astype(f32)
        else:
            mixed[...] = current + branch

    for c in sends:
        c.wait_send()


def update(state, forget, key, value, out):
    heads, size = state.shape[2], state.shape[3]
    for h in range(heads):
        cols = slice(h * size, (h + 1) * size)
        f_t = forget[0, :, cols].T
        k_t = key[0, :, cols].T
        v = value[0, :, cols]
        for j in range(GROUP):
            out[0, j, h] = f_t[:, j : j + 1] * state[0, j, h] + k_t[:, j : j + 1] * v[j : j + 1, :]


def shards(n_tp, n_dp, tokens, state, lengths, gain, w_query, w_forget, w_input, w_gate, w_out, bound, pace, head_gain):
    rt, feats = tokens.shape
    own, heads, size = state.shape[1:4]
    chans = heads * size
    rows = rt * n_tp
    msg = 4 * chans + 128
    vmem = pl.BlockSpec(memory_space=pltpu.VMEM)
    hbm = pl.BlockSpec(memory_space=pl.ANY)
    gates = jax.ShapeDtypeStruct((2, own, chans), f32)
    dma = pltpu.SemaphoreType.DMA
    mixed, forget, key, value = pl.pallas_call(
        functools.partial(chain, n_tp, n_dp, feats * n_dp),
        name="chain",
        out_shape=(jax.ShapeDtypeStruct((rt, feats), f32), gates, gates, gates),
        in_specs=[vmem, hbm, vmem, vmem] + [hbm] * 5 + [vmem] * 3,
        out_specs=(vmem,) * 4,
        scratch_shapes=[
            pltpu.VMEM((2, rows, feats), bf16),
            pltpu.VMEM((2, own, heads, size, size), f32),
            pltpu.VMEM((2, 4, feats, chans), bf16),
            pltpu.VMEM((2, chans, feats), bf16),
            pltpu.VMEM((2, n_dp - 1, own, msg), bf16),
            pltpu.VMEM((2, n_dp - 1, own, msg), bf16),
            pltpu.VMEM((own, 4 * chans), f32),
            pltpu.VMEM((2, rows, chans), bf16),
            pltpu.VMEM((2, n_tp - 1, rt, feats), bf16),
            pltpu.VMEM((2, n_tp - 1, rt, feats), bf16),
            pltpu.VMEM((rt, feats), f32),
            pltpu.VMEM((own, chans), f32),
            pltpu.VMEM((own, chans), f32),
            pltpu.VMEM((own, chans), f32),
            pltpu.VMEM((own, chans), f32),
            dma((2, 5)),
            dma((2, own // GROUP)),
            dma((2, n_tp - 1)),
            dma((2, n_tp - 1)),
            dma((2, n_dp - 1)),
            dma((2, n_dp - 1)),
            dma((2, n_dp - 1)),
            dma((2, n_dp - 1)),
            dma((2, n_tp - 1)),
            dma((2, n_tp - 1)),
        ],
        compiler_params=pltpu.CompilerParams(
            collective_id=0, has_side_effects=True, vmem_limit_bytes=60 * 1024 * 1024
        ),
    )(tokens, state, lengths[:, None], gain, w_query, w_forget, w_input, w_gate, w_out, bound, pace, head_gain)

    block = pl.BlockSpec((1, GROUP, heads, size, size), lambda b, g: (b, g, 0, 0, 0))
    row = pl.BlockSpec((1, GROUP, chans), lambda b, g: (b, g, 0))
    new_state = pl.pallas_call(
        update,
        name="update",
        grid=(2, own // GROUP),
        out_shape=jax.ShapeDtypeStruct(state.shape, f32),
        in_specs=[block, row, row, row],
        out_specs=block,
    )(state, forget, key, value)
    return mixed, new_state


def solution(mesh):
    in_specs = (
        P(("grp", "tp"), "dp"),
        P(None, ("grp", "dp"), "tp", None, None),
        P(("grp", "dp")),
        P(None, "dp"),
        P(None, "dp", "tp"),
        P(None, "dp", "tp"),
        P(None, "dp", "tp"),
        P(None, "dp", "tp"),
        P(None, "tp", "dp"),
        P(None, "tp"),
        P(None, "tp"),
        P(),
    )
    out_specs = (P(("grp", "tp"), "dp"), P(None, ("grp", "dp"), "tp", None, None))
    body = functools.partial(shards, mesh.shape["tp"], mesh.shape["dp"])
    return jax.shard_map(body, mesh=mesh, in_specs=in_specs, out_specs=out_specs, check_vma=False)
```

time: 362 us -> 126 us (0.35)
  waiting for transfers between devices: 161 us -> 0 us
  Pallas kernels: 0 us -> 123 us
  blocking collectives: 64.5 us -> 0 us
  matrix products: 62.6 us -> 0 us
  other arithmetic: 54.8 us -> 0 us
  between operations: 14.5 us -> 0.65 us
    reduce_scatter x10 -> x0, waiting for transfers between devices: 161 us -> none  [the longest x8 141 us: shards(): sums = lax.psum_scatter(terms, 'dp', scatter_dimension=0, tiled=True)]
    pallas_call x0 -> x2, Pallas kernels: none -> 123 us  [the longest x1 89.7 us: shards(): pl.pallas_call(functools.partial(chain, n_tp, n_dp, feats * n_dp), name='...]
    dot_general x12 -> x0, matrix products: 62.6 us -> none  [the longest x2 45.3 us: advance(): jnp.einsum('bhk,bhkv->bhv', query.reshape(count, heads, size), updated, p...]
    all_gather x4 -> x0, blocking collectives: 40.8 us -> none  [the longest x2 27.6 us: shards(): gathered = lax.all_gather(normed, 'dp', axis=0, tiled=True)]
    add x4 -> x0, other arithmetic: 27.3 us -> none  [the longest x1 23.2 us: advance(): updated = forget[..., None] * prior + key[..., None] * values[:, :, None, :]]
    psum x2 -> x0, blocking collectives: 23.7 us -> none  [shards(): squares_all = lax.psum(partial_sq, 'dp')]
    another operation x1 -> x0, other arithmetic: 23.4 us -> none  [shards(): return (result, jnp.stack(states))]
  transfers between devices with their start and end apart: 10 -> 0, of which waited for: 9 -> 0; matrix products, arithmetic and copies ran while one was open for 11% -> 0% of each run, Pallas kernels for 0% -> 0%
where the time goes in v1:
time: 126 us
  Pallas kernels  123 us (98%)
  local copies, waits for them, and re-layouts  2.02 us (2%)
    pallas_call x1, Pallas kernels, shards(): pl.pallas_call(functools.partial(chain, n_tp, n_dp, feats * n_dp), name='...  89.7 us
    pallas_call x1, Pallas kernels, shards(): pl.pallas_call(update, name='update', grid=(2, own // GROUP), out_shape=j...  33.5 us

profile of v1, /device:TPU:0, one launch (start us, length us, event | category | flops | bytes accessed | tf_op | source)
XLA Modules:
  0.0 125.8 jit_solution(468420342019145440)
XLA Ops:
  0.6 1.4 %copy.14.lengths = s32[64,1]{1,0:T(8,128)} copy(s32[64,1]{0,1:T(1,128)} %bitcast.1) | data formatting | bytes 512 | tf_op jit(solution)/shard_map/broadcast_in_dim | solution.py:325
  2.0 89.7 %chain.1 = (f32[64,512]{1,0:T(8,128)}, f32[2,64,512]{2,1,0:T(8,128)}, f32[2,64,512]{2,1,0:T(8,128)}, f32[2,64,512]{2,1,0:T(8,128)}) custom-call(bf16[64,512]{1,0:T(8,128)(2,1)} %tokens.1, f32[2,64,4,128,128]{4,3,2,1,0:T(8,128)} %state.3, s32[64,1]{1,0:T(8,128)} %copy.14.lengths, bf16[2,512]{1,0:T(2,128)(2,1)} %gain.1, bf16[2,512,512]{2,1,0:T(8,128)(2,1)} %w_query.1, ...), custom_call_target="tpu_custom_call" | custom-call | tf_op jit(solution)/shard_map/chain/pallas_call | solution.py:289
  91.7 0.0 copy-start
  91.7 33.5 %update.1 = f32[2,64,4,128,128]{4,3,2,1,0:T(8,128)} custom-call(f32[2,64,4,128,128]{4,3,2,1,0:T(8,128)} %state.3, f32[2,64,512]{2,1,0:T(8,128)} %get-tuple-element.7.forget, f32[2,64,512]{2,1,0:T(8,128)} %get-tuple-element.8.key, f32[2,64,512]{2,1,0:T(8,128)} %get-tuple-element.9.value), custom_call_target="tpu_custom_call" | custom-call | tf_op jit(solution)/shard_map/update/pallas_call | solution.py:329
  125.2 0.0 copy-done
  125.2 0.7 copy.16
Async XLA Ops:
  91.7 33.5 %copy-start = (f32[64,512]{1,0:T(8,128)S(1)}, f32[64,512]{1,0:T(8,128)}, u32[]{:S(2)}) copy-start(f32[64,512]{1,0:T(8,128)} %get-tuple-element.12) | copy-start | bytes 393220

commit v2 on v1

--- a/solution.py
+++ b/solution.py
@@ -10,6 +10,7 @@
 LENGTH_MEAN = 512
 epsilon = 1e-06
 GROUP = 8
+LIMIT = 26 * 1024 * 1024
 MESH_ID = pl.DeviceIdType.MESH
 f32 = jnp.float32
 bf16 = jnp.bfloat16
@@ -32,11 +33,11 @@
     pace,
     head_gain,
     mixed,
+    sbuf,
     forget_o,
     key_o,
     value_o,
     xall,
-    sbuf,
     wbuf,
     wobuf,
     psend,
@@ -102,6 +103,18 @@
     log_len = jnp.log(lengths[...].astype(f32) / LENGTH_MEAN)
     lane = lax.broadcasted_iota(jnp.int32, (own, 128), 1)
     row_id = lax.broadcasted_iota(jnp.int32, (GROUP, size), 0)
+
+    def advance(b, g, carry):
+        rows = pl.ds(pl.multiple_of(g * GROUP, GROUP), GROUP)
+        for h in range(heads):
+            cols = slice(h * size, (h + 1) * size)
+            f_t = forget_o[b, rows, cols].T
+            k_t = key_o[b, rows, cols].T
+            v = value_o[b, rows, cols]
+            for j in range(GROUP):
+                at = g * GROUP + j
+                sbuf[b, at, h] = f_t[:, j : j + 1] * sbuf[b, at, h] + k_t[:, j : j + 1] * v[j : j + 1, :]
+        return carry
 
     for b in range(2):
         copies = []
@@ -160,6 +173,8 @@
                 c.start()
                 copies.append(c)
         sends += copies
+        if b == 1:
+            lax.fori_loop(0, groups, functools.partial(advance, 0), 0)
         for c in copies:
             c.wait_recv()
 
@@ -226,6 +241,8 @@
             copies.append(c)
         sends += copies
         loads[b][4].wait()
+        if b == 1:
+            lax.fori_loop(0, groups, functools.partial(advance, 1), 0)
         for c in copies:
             c.wait_recv()
 
@@ -265,15 +282,17 @@
         c.wait_send()
 
 
-def update(state, forget, key, value, out):
-    heads, size = state.shape[2], state.shape[3]
-    for h in range(heads):
-        cols = slice(h * size, (h + 1) * size)
-        f_t = forget[0, :, cols].T
-        k_t = key[0, :, cols].T
-        v = value[0, :, cols]
-        for j in range(GROUP):
-            out[0, j, h] = f_t[:, j : j + 1] * state[0, j, h] + k_t[:, j : j + 1] * v[j : j + 1, :]
+def store(mixed, new_state, mixed_out, state_out, sems):
+    blocks, own = new_state.shape[:2]
+    copies = [pltpu.make_async_copy(mixed, mixed_out, sems.at[blocks, 0])]
+    for b in range(blocks):
+        for g in range(own // GROUP):
+            rows = pl.ds(g * GROUP, GROUP)
+            copies.append(pltpu.make_async_copy(new_state.at[b, rows], state_out.at[b, rows], sems.at[b, g]))
+    for c in copies:
+        c.start()
+    for c in copies:
+        c.wait()
 
 
 def shards(n_tp, n_dp, tokens, state, lengths, gain, w_query, w_forget, w_input, w_gate, w_out, bound, pace, head_gain):
@@ -284,17 +303,19 @@
     msg = 4 * chans + 128
     vmem = pl.BlockSpec(memory_space=pltpu.VMEM)
     hbm = pl.BlockSpec(memory_space=pl.ANY)
-    gates = jax.ShapeDtypeStruct((2, own, chans), f32)
+    gates = pltpu.VMEM((2, own, chans), f32)
     dma = pltpu.SemaphoreType.DMA
-    mixed, forget, key, value = pl.pallas_call(
+    mixed, new_state = pl.pallas_call(
         functools.partial(chain, n_tp, n_dp, feats * n_dp),
         name="chain",
-        out_shape=(jax.ShapeDtypeStruct((rt, feats), f32), gates, gates, gates),
+        out_shape=(pltpu.VMEM((rt, feats), f32), pltpu.VMEM(state.shape, f32)),
         in_specs=[vmem, hbm, vmem, vmem] + [hbm] * 5 + [vmem] * 3,
-        out_specs=(vmem,) * 4,
+        out_specs=(vmem, vmem),
         scratch_shapes=[
+            gates,
+            gates,
+            gates,
             pltpu.VMEM((2, rows, feats), bf16),
-            pltpu.VMEM((2, own, heads, size, size), f32),
             pltpu.VMEM((2, 4, feats, chans), bf16),
             pltpu.VMEM((2, chans, feats), bf16),
             pltpu.VMEM((2, n_dp - 1, own, msg), bf16),
@@ -320,21 +341,19 @@
             dma((2, n_tp - 1)),
         ],
         compiler_params=pltpu.CompilerParams(
-            collective_id=0, has_side_effects=True, vmem_limit_bytes=60 * 1024 * 1024
+            collective_id=0, has_side_effects=True, vmem_limit_bytes=LIMIT
         ),
     )(tokens, state, lengths[:, None], gain, w_query, w_forget, w_input, w_gate, w_out, bound, pace, head_gain)
 
-    block = pl.BlockSpec((1, GROUP, heads, size, size), lambda b, g: (b, g, 0, 0, 0))
-    row = pl.BlockSpec((1, GROUP, chans), lambda b, g: (b, g, 0))
-    new_state = pl.pallas_call(
-        update,
-        name="update",
-        grid=(2, own // GROUP),
-        out_shape=jax.ShapeDtypeStruct(state.shape, f32),
-        in_specs=[block, row, row, row],
-        out_specs=block,
-    )(state, forget, key, value)
-    return mixed, new_state
+    return pl.pallas_call(
+        store,
+        name="store",
+        out_shape=(jax.ShapeDtypeStruct((rt, feats), f32), jax.ShapeDtypeStruct(state.shape, f32)),
+        in_specs=[vmem, vmem],
+        out_specs=(hbm, hbm),
+        scratch_shapes=[dma((3, own // GROUP))],
+        compiler_params=pltpu.CompilerParams(vmem_limit_bytes=LIMIT),
+    )(pltpu.with_memory_space_constraint(mixed, pltpu.VMEM), pltpu.with_memory_space_constraint(new_state, pltpu.VMEM))
 
 
 def solution(mesh):

time: 126 us -> 109 us (0.87)
  the two profiles are of different devices: /device:TPU:0 before, /device:TPU:23 now
where the time goes in v2:
time: 109 us
  Pallas kernels  107 us (98%)
  local copies, waits for them, and re-layouts  1.36 us (1%)
    pallas_call x1, Pallas kernels, shards(): pl.pallas_call(functools.partial(chain, n_tp, n_dp, feats * n_dp), name='...  95.7 us
    pallas_call x1, Pallas kernels, shards(): pl.pallas_call(store, name='store', out_shape=(jax.ShapeDtypeStruct((rt,...  11.2 us

profile of v2, /device:TPU:23, one launch (start us, length us, event | category | flops | bytes accessed | tf_op | source)
XLA Modules:
  0.0 108.8 jit_solution(16102932543065235536)
XLA Ops:
  0.6 1.4 %copy.14.lengths = s32[64,1]{1,0:T(8,128)} copy(s32[64,1]{0,1:T(1,128)} %bitcast.1) | data formatting | bytes 512 | tf_op jit(solution)/shard_map/broadcast_in_dim | solution.py:346
  2.0 95.7 %chain.1 = (f32[64,512]{1,0:T(8,128)S(1)}, f32[2,64,4,128,128]{4,3,2,1,0:T(8,128)S(1)}) custom-call(bf16[64,512]{1,0:T(8,128)(2,1)} %tokens.1, f32[2,64,4,128,128]{4,3,2,1,0:T(8,128)} %state.1, s32[64,1]{1,0:T(8,128)} %copy.14.lengths, bf16[2,512]{1,0:T(2,128)(2,1)} %gain.1, bf16[2,512,512]{2,1,0:T(8,128)(2,1)} %w_query.1, bf16[2,512,512]{2,1,0:T(8,128)(2,1)} %w_forget.1, ...), custom_call_target="tpu_custom_call" | custom-call | tf_op jit(solution)/shard_map/chain/pallas_call | solution.py:308
  97.7 11.2 %store.1 = (f32[64,512]{1,0:T(8,128)}, f32[2,64,4,128,128]{4,3,2,1,0:T(8,128)}) custom-call(f32[64,512]{1,0:T(8,128)S(1)} %get-tuple-element.4.mixed, f32[2,64,4,128,128]{4,3,2,1,0:T(8,128)S(1)} %get-tuple-element.5.new_state), custom_call_target="tpu_custom_call" | custom-call | tf_op jit(solution)/shard_map/store/pallas_call | solution.py:348
